TPU v7x, 32 devices: a whole 2x2x4 slice. The times are simulated.
32 devices in a mesh: rep: 2 (over x), fs: 8 (over z, y), tp: 2 (over core).
Axes of the slice: x: 2, y: 2, z: 4, core: 2. Of those that a mesh axis runs over, the one named last changes fastest.
Arguments:
- stream: bfloat16 [4096, 2048], P(('rep', 'fs'), 'tp'), may hold values from -6 to 6
- norm_gains: float32 [6, 2048], replicated, may hold values from 0.1 to 1.9
- w_gate: bfloat16 [2048, 5632], P('fs', 'tp'), may hold values from -0.125 to 0.125
- w_up: bfloat16 [2048, 5632], P('fs', 'tp'), may hold values from -0.125 to 0.125
- w_down: bfloat16 [5632, 2048], P('tp', 'fs'), may hold values from -0.109375 to 0.109375
- w_inner: bfloat16 [2048, 1024], P('fs', 'tp'), may hold values from -0.125 to 0.125
- w_bgate: bfloat16 [2048, 1024], P('fs', 'tp'), may hold values from -0.125 to 0.125
- w_cgate: bfloat16 [2048, 1024], P('fs', 'tp'), may hold values from -0.125 to 0.125
- conv_taps: float32 [3, 1024], P(None, 'tp'), may hold values from -3.5 to 3.5
- w_out: bfloat16 [1024, 2048], P('tp', 'fs'), may hold values from -0.25 to 0.25
Outputs:
- mixed: bfloat16 [4096, 2048], P(('rep', 'fs'), 'tp')
All inputs are finite; a program needn't handle non-finite values.
Results may differ from a plain program's by a relative error of at most 0.02.
Values may be sent and summed in bfloat16 or wider, within the bound.
A program may use at most 128 MiB of HBM per device.

v0:
```python
import jax
import jax.numpy as jnp
from jax import lax
from jax.sharding import PartitionSpec as P

TAPS = 3
EPSILON = 1e-06


def from_behind(x, axis, by):
    count = lax.axis_size(axis)
    pairs = [(i, i + by) for i in range(count) if 0 <= i + by < count]
    return lax.ppermute(x, axis, pairs)


def shards(stream, norm_gains, w_gate, w_up, w_down, w_inner, w_bgate, w_cgate, conv_taps, w_out):
    tp_index = lax.axis_index("tp")
    local_width = stream.shape[1]
    model_width = local_width * lax.axis_size("tp")

    def own_gain(row):
        return lax.dynamic_slice_in_dim(norm_gains[row], tp_index * local_width, local_width, 0)

    def gathered_norm(current, row):
        gathered = lax.all_gather(current, "tp", axis=1, tiled=True)
        values = gathered.astype(jnp.float32)
        scaled = values * lax.rsqrt(jnp.mean(values * values, axis=1, keepdims=True) + EPSILON)
        return (scaled * norm_gains[row]).astype(jnp.bfloat16)

    def settle(current, partials, row, weight):
        branch_sum = lax.psum_scatter(
            partials.astype(jnp.bfloat16), "tp", scatter_dimension=1, tiled=True
        ).astype(jnp.float32)
        squares = lax.psum(jnp.sum(branch_sum * branch_sum, axis=1), "tp")
        scaled = branch_sum * lax.rsqrt(squares / model_width + EPSILON)[:, None]
        return (current.astype(jnp.float32) + weight * (scaled * own_gain(row))).astype(
            jnp.bfloat16
        )

    gate_whole, up_whole, down_whole = (
        lax.all_gather(w_gate, "fs", axis=0, tiled=True),
        lax.all_gather(w_up, "fs", axis=0, tiled=True),
        lax.all_gather(w_down, "fs", axis=1, tiled=True),
    )

    def feed_forward(current, row_in, row_out):
        normed = gathered_norm(current, row_in)
        gate_vals = jnp.dot(normed, gate_whole, preferred_element_type=jnp.float32)
        upward = jnp.dot(normed, up_whole, preferred_element_type=jnp.float32)
        hidden = (jax.nn.silu(gate_vals) * upward).astype(jnp.bfloat16)
        partials = jnp.dot(hidden, down_whole, preferred_element_type=jnp.float32)
        return settle(current, partials, row_out, 0.5)

    first = feed_forward(stream, 0, 1)
    normed_mix = gathered_norm(first, 2)
    local_rows = normed_mix.shape[0]

    def fold_rows(block_rows):
        return jnp.dot(normed_mix, block_rows, preferred_element_type=jnp.float32)

    inner = fold_rows(lax.all_gather(w_inner, "fs", axis=0, tiled=True))
    bgate = fold_rows(lax.all_gather(w_bgate, "fs", axis=0, tiled=True))
    cgate = fold_rows(lax.all_gather(w_cgate, "fs", axis=0, tiled=True))
    conv_input = cgate * inner
    earlier = from_behind(conv_input[local_rows - (TAPS - 1) :], "fs", 1)
    padded = jnp.concatenate([earlier, conv_input], axis=0)
    conv = conv_taps[0] * padded[0:local_rows]
    for tap in range(1, TAPS):
        conv = conv + conv_taps[tap] * padded[tap : tap + local_rows]
    gated = (bgate * conv).astype(jnp.bfloat16)
    mix_partials = jnp.dot(
        gated, lax.all_gather(w_out, "fs", axis=1, tiled=True), preferred_element_type=jnp.float32
    )
    second = settle(first, mix_partials, 3, 1.0)
    return feed_forward(second, 4, 5)


def solution(mesh):
    return jax.shard_map(
        shards,
        mesh=mesh,
        in_specs=(
            P(("rep", "fs"), "tp"),
            P(),
            P("fs", "tp"),
            P("fs", "tp"),
            P("tp", "fs"),
            P("fs", "tp"),
            P("fs", "tp"),
            P("fs", "tp"),
            P(None, "tp"),
            P("tp", "fs"),
        ),
        out_specs=P(("rep", "fs"), "tp"),
        check_vma=False,
    )
```

profile of v0, /device:TPU:0, one launch (start us, length us, event | category | flops | bytes accessed | tf_op | source)
XLA Modules:
  0.0 832.3 jit_solution(3071890299738791454)
XLA Ops:
  9.4 11.2 %all-gather.11.cloned.1.call-done = bf16[256,2048]{1,0:T(8,128)(2,1)} async-done(((bf16[256,1024]{1,0:T(8,128)(2,1)}), bf16[256,2048]{1,0:T(8,128)(2,1)}) %all-gather.11.cloned.1.call-update) | async-done | bytes 1048592 | tf_op jit(solution)/shard_map/all_gather | solution.py:25
  20.7 1.5 fusion.2
  22.2 165.2 %all-gather.13.cloned.1.call-done = bf16[2048,2816]{1,0:T(8,128)(2,1)} async-done(((bf16[256,2816]{1,0:T(8,128)(2,1)}), bf16[2048,2816]{1,0:T(8,128)(2,1)}) %all-gather.13.cloned.1.call-update) | async-done | bytes 11534352 | tf_op jit(solution)/shard_map/all_gather | solution.py:41
  187.4 9.5 %fusion.38 = f32[256,2816]{1,0:T(8,128)} fusion(bf16[2048,2816]{1,0:T(8,128)(2,1)} %all-gather.13.cloned.1.call-done, bf16[256,2048]{1,0:T(8,128)(2,1)} %all-gather.11.cloned.1.call-done, f32[2048]{0:T(1024)S(1)} %bitcast.27, f32[256]{0:T(256)S(1)} %add_rsqrt_fusion.5), kind=kOutput, calls=%fused_computation.54 | convolution fusion | flops 2954887168 | bytes 15475712 | tf_op jit(solution)/shard_map/dot_general | solution.py:48
  196.9 154.2 %all-gather.15.cloned.1.call-done = bf16[2048,2816]{1,0:T(8,128)(2,1)} async-done(((bf16[256,2816]{1,0:T(8,128)(2,1)}), bf16[2048,2816]{1,0:T(8,128)(2,1)}) %all-gather.15.cloned.1.call-update) | async-done | bytes 11534352 | tf_op jit(solution)/shard_map/all_gather | solution.py:42
  351.1 163.4 %all-gather.17.cloned.1.call-done = bf16[2816,2048]{1,0:T(8,128)(2,1)} async-done(((bf16[2816,256]{1,0:T(8,128)(2,1)}), bf16[2816,2048]{1,0:T(8,128)(2,1)}) %all-gather.17.cloned.1.call-update) | async-done | bytes 11534352 | tf_op jit(solution)/shard_map/all_gather | solution.py:43
  514.5 15.6 %convolution_convert_fusion.2 = bf16[256,2048]{1,0:T(8,128)(2,1)} fusion(bf16[2816,2048]{1,0:T(8,128)(2,1)} %all-gather.17.cloned.1.call-done, bf16[2048,2816]{1,0:T(8,128)(2,1)} %all-gather.15.cloned.1.call-done, f32[256,2816]{1,0:T(8,128)} %fusion.38, bf16[256,2048]{1,0:T(8,128)(2,1)S(1)} %copy-done.4, f32[2048]{0:T(1024)S(1)} %bitcast.28, ...), kind=kOutput, calls=%fused_computation.12 | convolution fusion | flops 5912526848 | bytes 28058624 | tf_op jit(solution)/shard_map/dot_general | solution.py:51
  530.2 6.6 reduce-scatter.4.cloned.1.call-done
  536.9 1.2 fusion.11
  538.1 2.5 psum.21
  540.6 2.1 fusion.15
  545.6 7.5 all-gather.19.cloned.1.call-done
  553.1 1.5 fusion.5
  554.6 50.9 %all-gather.23.cloned.1.call-done = bf16[2048,512]{1,0:T(8,128)(2,1)} async-done(((bf16[256,512]{1,0:T(8,128)(2,1)}), bf16[2048,512]{1,0:T(8,128)(2,1)}) %all-gather.23.cloned.1.call-update) | async-done | bytes 2097168 | tf_op jit(solution)/shard_map/all_gather | solution.py:63
  605.5 2.7 fusion.48
  608.3 47.0 %all-gather.25.cloned.1.call-done = bf16[2048,512]{1,0:T(8,128)(2,1)} async-done(((bf16[256,512]{1,0:T(8,128)(2,1)}), bf16[2048,512]{1,0:T(8,128)(2,1)}) %all-gather.25.cloned.1.call-update) | async-done | bytes 2097168 | tf_op jit(solution)/shard_map/all_gather | solution.py:61
  655.3 2.3 convolution_multiply_fusion.2
  657.6 2.5 collective-permute-start
  660.1 44.9 %all-gather.21.cloned.1.call-done = bf16[2048,512]{1,0:T(8,128)(2,1)} async-done(((bf16[256,512]{1,0:T(8,128)(2,1)}), bf16[2048,512]{1,0:T(8,128)(2,1)}) %all-gather.21.cloned.1.call-update) | async-done | bytes 2097168 | tf_op jit(solution)/shard_map/all_gather | solution.py:62
  705.1 50.8 %all-gather.27.cloned.1.call-done = bf16[512,2048]{1,0:T(8,128)(2,1)} async-done(((bf16[512,256]{1,0:T(8,128)(2,1)}), bf16[512,2048]{1,0:T(8,128)(2,1)}) %all-gather.27.cloned.1.call-update) | async-done | bytes 2097168 | tf_op jit(solution)/shard_map/all_gather | solution.py:72
  755.9 4.7 convolution_convert_fusion.1
  760.6 6.7 reduce-scatter.6.cloned.1.call-done
  768.5 2.5 psum.22
  771.0 2.1 fusion.19
  773.4 10.1 %all-gather.29.cloned.1.call-done = bf16[256,2048]{1,0:T(8,128)(2,1)} async-done(((bf16[256,1024]{1,0:T(8,128)(2,1)}), bf16[256,2048]{1,0:T(8,128)(2,1)}) %all-gather.29.cloned.1.call-update) | async-done | bytes 1048592 | tf_op jit(solution)/shard_map/all_gather | solution.py:25
  783.5 1.5 fusion.8
  785.0 9.5 %fusion.34 = f32[256,2816]{1,0:T(8,128)} fusion(bf16[2048,2816]{1,0:T(8,128)(2,1)} %all-gather.13.cloned.1.call-done, bf16[256,2048]{1,0:T(8,128)(2,1)} %all-gather.29.cloned.1.call-done, f32[2048]{0:T(1024)S(1)} %bitcast.22, f32[256]{0:T(256)S(1)} %add_rsqrt_fusion.1), kind=kOutput, calls=%fused_computation.53 | convolution fusion | flops 2954887168 | bytes 15475712 | tf_op jit(solution)/shard_map/dot_general | solution.py:48
  794.5 15.7 %convolution_convert_fusion = bf16[256,2048]{1,0:T(8,128)(2,1)} fusion(bf16[2816,2048]{1,0:T(8,128)(2,1)} %all-gather.17.cloned.1.call-done, bf16[2048,2816]{1,0:T(8,128)(2,1)} %all-gather.15.cloned.1.call-done, f32[256,2816]{1,0:T(8,128)} %fusion.34, bf16[256,2048]{1,0:T(8,128)(2,1)S(1)} %copy-done.5, f32[2048]{0:T(1024)S(1)} %bitcast.23, ...), kind=kOutput, calls=%fused_computation.10 | convolution fusion | flops 5912526848 | bytes 28058624 | tf_op jit(solution)/shard_map/dot_general | solution.py:51
  810.3 9.7 %reduce-scatter.8.cloned.1.call-done = bf16[256,1024]{1,0:T(8,128)(2,1)} async-done(((bf16[256,2048]{1,0:T(8,128)(2,1)}), bf16[256,1024]{1,0:T(8,128)(2,1)}) %reduce-scatter.8.cloned.1.call-update) | async-done | bytes 524304 | tf_op jit(solution)/shard_map/reduce_scatter | solution.py:31
  820.0 1.2 fusion.20
  821.2 2.5 psum.23
  823.7 2.1 fusion.24
  (56 shorter events, 7.3 us)
Async XLA Ops:
  6.5 14.1 %all-gather.11.cloned.1.call-start = ((), (), s32[]{:S(2)}) async-start(), calls=%async_computation.3 | async-start | bytes 1572864 | tf_op jit(solution)/shard_map/all_gather | solution.py:25
  7.3 2.1 copy-start.6
  7.3 180.1 %all-gather.13.cloned.1.call-start = ((), (), s32[]{:S(2)}) async-start(), calls=%async_computation.4 | async-start | bytes 12976128 | tf_op jit(solution)/shard_map/all_gather | solution.py:41
  8.0 343.1 %all-gather.15.cloned.1.call-start = ((), (), s32[]{:S(2)}) async-start(), calls=%async_computation.5 | async-start | bytes 12976128 | tf_op jit(solution)/shard_map/all_gather | solution.py:42
  8.8 505.8 %all-gather.17.cloned.1.call-start = ((), (), s32[]{:S(2)}) async-start(), calls=%async_computation.6 | async-start | bytes 12976128 | tf_op jit(solution)/shard_map/all_gather | solution.py:43
  9.3 527.5 %reduce-scatter.4.cloned.1.call-start = ((), (), s32[]{:S(2)}) async-start(), calls=%async_computation.7 | async-start | bytes 1572864 | tf_op jit(solution)/shard_map/reduce_scatter | solution.py:31
  187.4 327.2 %copy-start.4 = (bf16[256,2048]{1,0:T(8,128)(2,1)S(1)}, bf16[256,2048]{1,0:T(8,128)(2,1)}, u32[]{:S(2)}) copy-start(bf16[256,2048]{1,0:T(8,128)(2,1)} %all-gather.11.cloned.1.call-done) | copy-start | bytes 3145732
  196.9 343.7 %copy-start.2 = (bf16[256,1024]{1,0:T(8,128)(2,1)S(1)}, bf16[256,1024]{1,0:T(8,128)(2,1)}, u32[]{:S(2)}) copy-start(bf16[256,1024]{1,0:T(8,128)(2,1)} %param.10) | copy-start | bytes 1572868
  530.2 22.9 %all-gather.19.cloned.1.call-start = ((), (), s32[]{:S(2)}) async-start(), calls=%async_computation.8 | async-start | bytes 1572864 | tf_op jit(solution)/shard_map/all_gather | solution.py:25
  542.7 62.8 %all-gather.23.cloned.1.call-start = ((), (), s32[]{:S(2)}) async-start(), calls=%async_computation.10 | async-start | bytes 2359296 | tf_op jit(solution)/shard_map/all_gather | solution.py:63
  543.5 111.8 %all-gather.25.cloned.1.call-start = ((), (), s32[]{:S(2)}) async-start(), calls=%async_computation.11 | async-start | bytes 2359296 | tf_op jit(solution)/shard_map/all_gather | solution.py:61
  544.2 160.8 %all-gather.21.cloned.1.call-start = ((), (), s32[]{:S(2)}) async-start(), calls=%async_computation.9 | async-start | bytes 2359296 | tf_op jit(solution)/shard_map/all_gather | solution.py:62
  545.0 210.9 %all-gather.27.cloned.1.call-start = ((), (), s32[]{:S(2)}) async-start(), calls=%async_computation.12 | async-start | bytes 2359296 | tf_op jit(solution)/shard_map/all_gather | solution.py:72
  545.6 221.8 %reduce-scatter.6.cloned.1.call-start = ((), (), s32[]{:S(2)}) async-start(), calls=%async_computation.13 | async-start | bytes 1572864 | tf_op jit(solution)/shard_map/reduce_scatter | solution.py:31
  605.5 49.8 %copy-start.3 = (bf16[256,2048]{1,0:T(8,128)(2,1)S(1)}, bf16[256,2048]{1,0:T(8,128)(2,1)}, u32[]{:S(2)}) copy-start(bf16[256,2048]{1,0:T(8,128)(2,1)} %all-gather.19.cloned.1.call-done) | copy-start | bytes 3145732
  608.3 51.9 %copy-start.7 = (f32[3,512]{1,0:T(4,128)S(1)}, f32[3,512]{1,0:T(4,128)}, u32[]{:S(2)}) copy-start(f32[3,512]{1,0:T(4,128)} %param.18) | copy-start | bytes 18436
  657.6 98.2 %collective-permute-start = (f32[2,512]{1,0:T(2,128)S(1)}, f32[2,512]{1,0:T(2,128)S(1)}, u32[]{:S(2)}, u32[]{:S(2)}) collective-permute-start(f32[2,512]{1,0:T(2,128)S(1)} %slice.48), channel_id=1, source_target_pairs={{0,2},{2,4},{4,6},{6,8},{8,10},{10,12},{12,14},{1,3},{3,5},{5,7},{... | collective-permute-start | bytes 12296 | tf_op jit(solution)/shard_map/ppermute | solution.py:13
  755.9 15.1 %copy-start = (bf16[256,1024]{1,0:T(8,128)(2,1)S(1)}, bf16[256,1024]{1,0:T(8,128)(2,1)}, u32[]{:S(2)}) copy-start(bf16[256,1024]{1,0:T(8,128)(2,1)} %fusion.15) | copy-start | bytes 1572868
  760.6 22.9 %all-gather.29.cloned.1.call-start = ((), (), s32[]{:S(2)}) async-start(), calls=%async_computation.14 | async-start | bytes 1572864 | tf_op jit(solution)/shard_map/all_gather | solution.py:25
  773.1 46.8 %reduce-scatter.8.cloned.1.call-start = ((), (), s32[]{:S(2)}) async-start(), calls=%async_computation.15 | async-start | bytes 1572864 | tf_op jit(solution)/shard_map/reduce_scatter | solution.py:31
  785.0 9.5 %copy-start.5 = (bf16[256,2048]{1,0:T(8,128)(2,1)S(1)}, bf16[256,2048]{1,0:T(8,128)(2,1)}, u32[]{:S(2)}) copy-start(bf16[256,2048]{1,0:T(8,128)(2,1)} %all-gather.29.cloned.1.call-done) | copy-start | bytes 3145732
  794.5 29.1 %copy-start.1 = (bf16[256,1024]{1,0:T(8,128)(2,1)S(1)}, bf16[256,1024]{1,0:T(8,128)(2,1)}, u32[]{:S(2)}) copy-start(bf16[256,1024]{1,0:T(8,128)(2,1)} %fusion.19) | copy-start | bytes 1572868
Sparse Core Ops, SparseCore 0:
  8.9 11.7 all-gather.10
  22.8 164.4 all-gather.12
  189.6 161.4 all-gather.14
  353.0 161.4 all-gather.16
  530.3 6.5 reduce-scatter.3
  542.8 10.1 all-gather.18
  555.2 50.2 all-gather.22
  607.6 47.6 all-gather.24
  657.4 47.6 all-gather.20
  706.9 48.8 all-gather.26
  760.7 6.5 reduce-scatter.5
  773.2 10.1 all-gather.28
  810.4 9.5 reduce-scatter.7
where the time goes:
time: 833 us; the launch traced here: 832 us
  waiting for transfers between devices  734 us (88%)
  matrix products  60.1 us (7%)
  other arithmetic  14.6 us (2%)
  between operations  13.4 us (2%)
    all_gather x1, waiting for transfers between devices, shards(): lax.all_gather(w_gate, 'fs', axis=0, tiled=True)  165 us
    all_gather x1, waiting for transfers between devices, shards(): lax.all_gather(w_down, 'fs', axis=1, tiled=True)  163 us
    all_gather x1, waiting for transfers between devices, shards(): lax.all_gather(w_up, 'fs', axis=0, tiled=True)  154 us
    all_gather x1, waiting for transfers between devices, shards(): cgate = fold_rows(lax.all_gather(w_cgate, 'fs', axis=0, tiled=True))  50.9 us
    all_gather x1, waiting for transfers between devices, shards(): lax.all_gather(w_out, 'fs', axis=1, tiled=True)  50.8 us
    all_gather x1, waiting for transfers between devices, shards(): inner = fold_rows(lax.all_gather(w_inner, 'fs', axis=0, tiled=True))  47 us
    all_gather x1, waiting for transfers between devices, shards(): bgate = fold_rows(lax.all_gather(w_bgate, 'fs', axis=0, tiled=True))  44.9 us
    dot_general x2, matrix products, feed_forward(): partials = jnp.dot(hidden, down_whole, preferred_element_type=jnp.float32)  31.3 us
  transfers between devices with their start and end apart: 14, of which 13 were waited for; matrix products, arithmetic and copies ran while one was open for 2% of the time, Pallas kernels for 0%

commit v1 on v0

--- a/solution.py
+++ b/solution.py
@@ -69,7 +69,9 @@
         conv = conv + conv_taps[tap] * padded[tap : tap + local_rows]
     gated = (bgate * conv).astype(jnp.bfloat16)
     mix_partials = jnp.dot(
-        gated, lax.all_gather(w_out, "fs", axis=1, tiled=True), preferred_element_type=jnp.float32
+        gated,
+        jnp.concatenate(lax.all_gather(w_out, "fs"), axis=1),
+        preferred_element_type=jnp.float32,
     )
     second = settle(first, mix_partials, 3, 1.0)
     return feed_forward(second, 4, 5)

time: 833 us -> 832 us (level)
  no operation moved by 1% of the time
where the time goes in v1:
time: 832 us; the launch traced here: 831 us
  waiting for transfers between devices  730 us (88%)
  matrix products  59.9 us (7%)
  other arithmetic  14.6 us (2%)
  between operations  13.4 us (2%)
    all_gather x1, waiting for transfers between devices, shards(): lax.all_gather(w_gate, 'fs', axis=0, tiled=True)  165 us
    all_gather x1, waiting for transfers between devices, shards(): lax.all_gather(w_down, 'fs', axis=1, tiled=True)  163 us
    all_gather x1, waiting for transfers between devices, shards(): lax.all_gather(w_up, 'fs', axis=0, tiled=True)  154 us
    all_gather x1, waiting for transfers between devices, shards(): cgate = fold_rows(lax.all_gather(w_cgate, 'fs', axis=0, tiled=True))  50.9 us
    all_gather x1, waiting for transfers between devices, shards(): inner = fold_rows(lax.all_gather(w_inner, 'fs', axis=0, tiled=True))  47 us
    all_gather x1, waiting for transfers between devices, shards(): bgate = fold_rows(lax.all_gather(w_bgate, 'fs', axis=0, tiled=True))  46.8 us
    all_gather x1, waiting for transfers between devices, shards(): lax.all_gather(w_out, 'fs')  44.9 us
    dot_general x2, matrix products, feed_forward(): partials = jnp.dot(hidden, down_whole, preferred_element_type=jnp.float32)  31.3 us
  transfers between devices with their start and end apart: 14, of which 13 were waited for; matrix products, arithmetic and copies ran while one was open for 2% of the time, Pallas kernels for 0%

profile of v1, /device:TPU:0, one launch (start us, length us, event | category | flops | bytes accessed | tf_op | source)
XLA Modules:
  0.0 831.2 jit_solution(13158161976948752682)
XLA Ops:
  9.4 11.2 %all-gather.12.cloned.1.call-done = bf16[256,2048]{1,0:T(8,128)(2,1)} async-done(((bf16[256,1024]{1,0:T(8,128)(2,1)}), bf16[256,2048]{1,0:T(8,128)(2,1)}) %all-gather.12.cloned.1.call-update) | async-done | bytes 1048592 | tf_op jit(solution)/shard_map/all_gather | solution.py:25
  20.7 1.5 fusion.2
  22.2 165.2 %all-gather.14.cloned.1.call-done = bf16[2048,2816]{1,0:T(8,128)(2,1)} async-done(((bf16[256,2816]{1,0:T(8,128)(2,1)}), bf16[2048,2816]{1,0:T(8,128)(2,1)}) %all-gather.14.cloned.1.call-update) | async-done | bytes 11534352 | tf_op jit(solution)/shard_map/all_gather | solution.py:41
  187.4 9.5 %fusion.38 = f32[256,2816]{1,0:T(8,128)} fusion(bf16[2048,2816]{1,0:T(8,128)(2,1)} %all-gather.14.cloned.1.call-done, bf16[256,2048]{1,0:T(8,128)(2,1)} %all-gather.12.cloned.1.call-done, f32[2048]{0:T(1024)S(1)} %bitcast.33, f32[256]{0:T(256)S(1)} %add_rsqrt_fusion.5), kind=kOutput, calls=%fused_computation.54 | convolution fusion | flops 2954887168 | bytes 15475712 | tf_op jit(solution)/shard_map/dot_general | solution.py:48
  196.9 154.2 %all-gather.16.cloned.1.call-done = bf16[2048,2816]{1,0:T(8,128)(2,1)} async-done(((bf16[256,2816]{1,0:T(8,128)(2,1)}), bf16[2048,2816]{1,0:T(8,128)(2,1)}) %all-gather.16.cloned.1.call-update) | async-done | bytes 11534352 | tf_op jit(solution)/shard_map/all_gather | solution.py:42
  351.1 163.4 %all-gather.18.cloned.1.call-done = bf16[2816,2048]{1,0:T(8,128)(2,1)} async-done(((bf16[2816,256]{1,0:T(8,128)(2,1)}), bf16[2816,2048]{1,0:T(8,128)(2,1)}) %all-gather.18.cloned.1.call-update) | async-done | bytes 11534352 | tf_op jit(solution)/shard_map/all_gather | solution.py:43
  514.5 15.6 %convolution_convert_fusion.2 = bf16[256,2048]{1,0:T(8,128)(2,1)} fusion(bf16[2816,2048]{1,0:T(8,128)(2,1)} %all-gather.18.cloned.1.call-done, bf16[2048,2816]{1,0:T(8,128)(2,1)} %all-gather.16.cloned.1.call-done, f32[256,2816]{1,0:T(8,128)} %fusion.38, bf16[256,2048]{1,0:T(8,128)(2,1)S(1)} %copy-done.4, f32[2048]{0:T(1024)S(1)} %bitcast.34, ...), kind=kOutput, calls=%fused_computation.12 | convolution fusion | flops 5912526848 | bytes 28058624 | tf_op jit(solution)/shard_map/dot_general | solution.py:51
  530.2 6.6 reduce-scatter.4.cloned.1.call-done
  538.1 2.5 psum.21
  540.6 2.1 fusion.15
  545.6 7.5 all-gather.20.cloned.1.call-done
  553.1 1.5 fusion.5
  554.6 50.9 %all-gather.24.cloned.1.call-done = bf16[2048,512]{1,0:T(8,128)(2,1)} async-done(((bf16[256,512]{1,0:T(8,128)(2,1)}), bf16[2048,512]{1,0:T(8,128)(2,1)}) %all-gather.24.cloned.1.call-update) | async-done | bytes 2097168 | tf_op jit(solution)/shard_map/all_gather | solution.py:63
  605.5 2.7 fusion.48
  608.3 47.0 %all-gather.26.cloned.1.call-done = bf16[2048,512]{1,0:T(8,128)(2,1)} async-done(((bf16[256,512]{1,0:T(8,128)(2,1)}), bf16[2048,512]{1,0:T(8,128)(2,1)}) %all-gather.26.cloned.1.call-update) | async-done | bytes 2097168 | tf_op jit(solution)/shard_map/all_gather | solution.py:61
  655.3 2.3 convolution_multiply_fusion.2
  657.6 2.5 collective-permute-start
  660.1 44.9 %all-gather.30.cloned.1.call-done = bf16[4096,256]{1,0:T(8,128)(2,1)} async-done(((bf16[512,256]{1,0:T(8,128)(2,1)}), bf16[4096,256]{1,0:T(8,128)(2,1)}) %all-gather.30.cloned.1.call-update) | async-done | bytes 2097168 | tf_op jit(solution)/shard_map/all_gather | solution.py:73
  705.1 2.9 copy.11
  707.9 46.8 %all-gather.22.cloned.1.call-done = bf16[2048,512]{1,0:T(8,128)(2,1)} async-done(((bf16[256,512]{1,0:T(8,128)(2,1)}), bf16[2048,512]{1,0:T(8,128)(2,1)}) %all-gather.22.cloned.1.call-update) | async-done | bytes 2097168 | tf_op jit(solution)/shard_map/all_gather | solution.py:62
  754.7 4.4 convolution_convert_fusion.1
  759.2 7.0 reduce-scatter.6.cloned.1.call-done
  766.2 1.2 fusion.16
  767.4 2.5 psum.22
  769.9 2.1 fusion.19
  772.3 10.1 %all-gather.28.cloned.1.call-done = bf16[256,2048]{1,0:T(8,128)(2,1)} async-done(((bf16[256,1024]{1,0:T(8,128)(2,1)}), bf16[256,2048]{1,0:T(8,128)(2,1)}) %all-gather.28.cloned.1.call-update) | async-done | bytes 1048592 | tf_op jit(solution)/shard_map/all_gather | solution.py:25
  782.4 1.5 fusion.8
  783.9 9.5 %fusion.34 = f32[256,2816]{1,0:T(8,128)} fusion(bf16[2048,2816]{1,0:T(8,128)(2,1)} %all-gather.14.cloned.1.call-done, bf16[256,2048]{1,0:T(8,128)(2,1)} %all-gather.28.cloned.1.call-done, f32[2048]{0:T(1024)S(1)} %bitcast.28, f32[256]{0:T(256)S(1)} %add_rsqrt_fusion.1), kind=kOutput, calls=%fused_computation.53 | convolution fusion | flops 2954887168 | bytes 15475712 | tf_op jit(solution)/shard_map/dot_general | solution.py:48
  793.4 15.7 %convolution_convert_fusion = bf16[256,2048]{1,0:T(8,128)(2,1)} fusion(bf16[2816,2048]{1,0:T(8,128)(2,1)} %all-gather.18.cloned.1.call-done, bf16[2048,2816]{1,0:T(8,128)(2,1)} %all-gather.16.cloned.1.call-done, f32[256,2816]{1,0:T(8,128)} %fusion.34, bf16[256,2048]{1,0:T(8,128)(2,1)S(1)} %copy-done.5, f32[2048]{0:T(1024)S(1)} %bitcast.29, ...), kind=kOutput, calls=%fused_computation.10 | convolution fusion | flops 5912526848 | bytes 28058624 | tf_op jit(solution)/shard_map/dot_general | solution.py:51
  809.2 9.7 %reduce-scatter.8.cloned.1.call-done = bf16[256,1024]{1,0:T(8,128)(2,1)} async-done(((bf16[256,2048]{1,0:T(8,128)(2,1)}), bf16[256,1024]{1,0:T(8,128)(2,1)}) %reduce-scatter.8.cloned.1.call-update) | async-done | bytes 524304 | tf_op jit(solution)/shard_map/reduce_scatter | solution.py:31
  820.1 2.5 psum.23
  822.6 2.1 fusion.24
  (57 shorter events, 8.6 us)
Async XLA Ops:
  6.5 14.1 %all-gather.12.cloned.1.call-start = ((), (), s32[]{:S(2)}) async-start(), calls=%async_computation.3 | async-start | bytes 1572864 | tf_op jit(solution)/shard_map/all_gather | solution.py:25
  7.3 2.1 copy-start.6
  7.3 180.1 %all-gather.14.cloned.1.call-start = ((), (), s32[]{:S(2)}) async-start(), calls=%async_computation.4 | async-start | bytes 12976128 | tf_op jit(solution)/shard_map/all_gather | solution.py:41
  8.0 343.1 %all-gather.16.cloned.1.call-start = ((), (), s32[]{:S(2)}) async-start(), calls=%async_computation.5 | async-start | bytes 12976128 | tf_op jit(solution)/shard_map/all_gather | solution.py:42
  8.8 505.8 %all-gather.18.cloned.1.call-start = ((), (), s32[]{:S(2)}) async-start(), calls=%async_computation.6 | async-start | bytes 12976128 | tf_op jit(solution)/shard_map/all_gather | solution.py:43
  9.3 527.5 %reduce-scatter.4.cloned.1.call-start = ((), (), s32[]{:S(2)}) async-start(), calls=%async_computation.7 | async-start | bytes 1572864 | tf_op jit(solution)/shard_map/reduce_scatter | solution.py:31
  187.4 327.2 %copy-start.4 = (bf16[256,2048]{1,0:T(8,128)(2,1)S(1)}, bf16[256,2048]{1,0:T(8,128)(2,1)}, u32[]{:S(2)}) copy-start(bf16[256,2048]{1,0:T(8,128)(2,1)} %all-gather.12.cloned.1.call-done) | copy-start | bytes 3145732
  196.9 343.7 %copy-start.2 = (bf16[256,1024]{1,0:T(8,128)(2,1)S(1)}, bf16[256,1024]{1,0:T(8,128)(2,1)}, u32[]{:S(2)}) copy-start(bf16[256,1024]{1,0:T(8,128)(2,1)} %param.10) | copy-start | bytes 1572868
  530.2 22.9 %all-gather.20.cloned.1.call-start = ((), (), s32[]{:S(2)}) async-start(), calls=%async_computation.8 | async-start | bytes 1572864 | tf_op jit(solution)/shard_map/all_gather | solution.py:25
  542.7 62.8 %all-gather.24.cloned.1.call-start = ((), (), s32[]{:S(2)}) async-start(), calls=%async_computation.10 | async-start | bytes 2359296 | tf_op jit(solution)/shard_map/all_gather | solution.py:63
  543.5 111.8 %all-gather.26.cloned.1.call-start = ((), (), s32[]{:S(2)}) async-start(), calls=%async_computation.11 | async-start | bytes 2359296 | tf_op jit(solution)/shard_map/all_gather | solution.py:61
  544.2 160.8 %all-gather.30.cloned.1.call-start = ((), (), s32[]{:S(2)}) async-start(), calls=%async_computation.15 | async-start | bytes 2359296 | tf_op jit(solution)/shard_map/all_gather | solution.py:73
  545.0 209.7 %all-gather.22.cloned.1.call-start = ((), (), s32[]{:S(2)}) async-start(), calls=%async_computation.9 | async-start | bytes 2359296 | tf_op jit(solution)/shard_map/all_gather | solution.py:62
  545.6 220.7 %reduce-scatter.6.cloned.1.call-start = ((), (), s32[]{:S(2)}) async-start(), calls=%async_computation.12 | async-start | bytes 1572864 | tf_op jit(solution)/shard_map/reduce_scatter | solution.py:31
  605.5 49.8 %copy-start.3 = (bf16[256,2048]{1,0:T(8,128)(2,1)S(1)}, bf16[256,2048]{1,0:T(8,128)(2,1)}, u32[]{:S(2)}) copy-start(bf16[256,2048]{1,0:T(8,128)(2,1)} %all-gather.20.cloned.1.call-done) | copy-start | bytes 3145732
  608.3 51.9 %copy-start.7 = (f32[3,512]{1,0:T(4,128)S(1)}, f32[3,512]{1,0:T(4,128)}, u32[]{:S(2)}) copy-start(f32[3,512]{1,0:T(4,128)} %param.18) | copy-start | bytes 18436
  657.6 97.1 %collective-permute-start = (f32[2,512]{1,0:T(2,128)S(1)}, f32[2,512]{1,0:T(2,128)S(1)}, u32[]{:S(2)}, u32[]{:S(2)}) collective-permute-start(f32[2,512]{1,0:T(2,128)S(1)} %slice.48), channel_id=1, source_target_pairs={{0,2},{2,4},{4,6},{6,8},{8,10},{10,12},{12,14},{1,3},{3,5},{5,7},{... | collective-permute-start | bytes 12296 | tf_op jit(solution)/shard_map/ppermute | solution.py:13
  754.7 15.2 %copy-start = (bf16[256,1024]{1,0:T(8,128)(2,1)S(1)}, bf16[256,1024]{1,0:T(8,128)(2,1)}, u32[]{:S(2)}) copy-start(bf16[256,1024]{1,0:T(8,128)(2,1)} %fusion.15) | copy-start | bytes 1572868
  759.2 23.2 %all-gather.28.cloned.1.call-start = ((), (), s32[]{:S(2)}) async-start(), calls=%async_computation.13 | async-start | bytes 1572864 | tf_op jit(solution)/shard_map/all_gather | solution.py:25
  772.0 46.8 %reduce-scatter.8.cloned.1.call-start = ((), (), s32[]{:S(2)}) async-start(), calls=%async_computation.14 | async-start | bytes 1572864 | tf_op jit(solution)/shard_map/reduce_scatter | solution.py:31
  783.9 9.5 %copy-start.5 = (bf16[256,2048]{1,0:T(8,128)(2,1)S(1)}, bf16[256,2048]{1,0:T(8,128)(2,1)}, u32[]{:S(2)}) copy-start(bf16[256,2048]{1,0:T(8,128)(2,1)} %all-gather.28.cloned.1.call-done) | copy-start | bytes 3145732
  793.4 29.1 %copy-start.1 = (bf16[256,1024]{1,0:T(8,128)(2,1)S(1)}, bf16[256,1024]{1,0:T(8,128)(2,1)}, u32[]{:S(2)}) copy-start(bf16[256,1024]{1,0:T(8,128)(2,1)} %fusion.19) | copy-start | bytes 1572868
Sparse Core Ops, SparseCore 0:
  8.9 11.7 all-gather.11
  22.8 164.4 all-gather.13
  189.6 161.4 all-gather.15
  353.0 161.4 all-gather.17
  530.3 6.5 reduce-scatter.3
  542.8 10.1 all-gather.19
  555.2 50.2 all-gather.23
  607.6 47.6 all-gather.25
  657.4 47.6 all-gather.29
  707.0 47.6 all-gather.21
  759.3 6.9 reduce-scatter.5
  772.2 10.1 all-gather.27
  809.3 9.5 reduce-scatter.7
